TPU v7x, 32 devices: a whole 2x2x4 slice. The times are simulated.
32 devices in a mesh: sp: 4 (over y, x), tp: 8 (over z, core).
Axes of the slice: x: 2, y: 2, z: 4, core: 2. Of those that a mesh axis runs over, the one named last changes fastest.
Arguments:
- conv_value: bfloat16 [6144, 2048], P('sp', 'tp'), may hold values from -48 to 48
- conv_gate: bfloat16 [6144, 2048], P('sp', 'tp'), may hold values from -6 to 6
- doc_ids: int32 [6144], P('sp'), may hold values from 0 to 3, never falling along the last dimension, each value on 1 to 4608 neighbouring positions
- conv_kernel: bfloat16 [31, 2048], P(None, 'tp'), may hold values from -1 to 1
- norm_gain_conv: float32 [2048], replicated, may hold values from 0.1 to 1.9
- norm_bias_conv: float32 [2048], replicated, may hold values from -3 to 3
- proj_weight: bfloat16 [2048, 2048], P('tp'), may hold values from -0.125 to 0.125
- residual: bfloat16 [6144, 2048], P(('sp', 'tp')), may hold values from -6 to 6
- norm_gain_moe: float32 [2048], replicated, may hold values from 0.1 to 1.9
- group_router: bfloat16 [2048, 2], replicated, may hold values from -0.125 to 0.125
- expert_router: bfloat16 [2048, 4], replicated, may hold values from -0.125 to 0.125
- routing: int32 [6144, 2], P(('sp', 'tp')), may hold values from 0 to 3, as said below
- expert_gate_w: bfloat16 [4, 2048, 512], P('sp'), may hold values from -0.125 to 0.125
- expert_up_w: bfloat16 [4, 2048, 512], P('sp'), may hold values from -0.125 to 0.125
- expert_down_w: bfloat16 [4, 512, 2048], P('sp'), may hold values from -0.25 to 0.25
Outputs:
- output: bfloat16 [6144, 2048], P(('sp', 'tp'))
Inputs may be any that keep to these rules, and one draw needn't show every extreme that they name: `routing`: both numbers of a row are different experts of one group (expert // 2); within the rows of one device (aligned blocks of 192 rows) every expert is named exactly 96 times.
All inputs are finite; a program needn't handle non-finite values.
Results may differ from a plain program's by a relative error of at most 0.015.
Values may be sent and summed in bfloat16 or wider, within the bound.
A program may use at most 64 MiB of HBM per device.

v0:
```python
import jax
import jax.numpy as jnp
from jax import lax
from jax.sharding import PartitionSpec as P

epsilon = 1e-06


def shifted(array, axis, by):
    count = lax.axis_size(axis)
    pairs = [(i, i + by) for i in range(count) if 0 <= i + by < count]
    return lax.ppermute(array, axis, pairs)


def normalize_channels(convolved, norm_gain_conv, norm_bias_conv, channel_start, total_width):
    local_width = convolved.shape[1]
    values = convolved.astype(jnp.float32)
    sum_values, sum_squares = lax.psum(
        (jnp.sum(values, axis=1), jnp.sum(values * values, axis=1)), "tp"
    )
    average = sum_values / total_width
    variance = sum_squares / total_width - average * average
    gain_slice = lax.dynamic_slice_in_dim(norm_gain_conv, channel_start, local_width)
    bias_slice = lax.dynamic_slice_in_dim(norm_bias_conv, channel_start, local_width)
    scaled = (values - average[:, None]) * lax.rsqrt(variance + epsilon)[:, None]
    return jax.nn.silu(scaled * gain_slice[None, :] + bias_slice[None, :]).astype(jnp.bfloat16)


def project_rows(activated_rows, proj_weight):
    return jnp.dot(
        activated_rows,
        lax.all_gather(proj_weight, "tp", axis=0, tiled=True),
        preferred_element_type=jnp.float32,
    )


def body(
    conv_value,
    conv_gate,
    doc_ids,
    conv_kernel,
    norm_gain_conv,
    norm_bias_conv,
    proj_weight,
    residual,
    norm_gain_moe,
    group_router,
    expert_router,
    routing,
    expert_gate_w,
    expert_up_w,
    expert_down_w,
):
    local_tokens, local_width = conv_value.shape
    kernel_taps = conv_kernel.shape[0]
    rim_width = kernel_taps - 1
    gated_values = (
        conv_value.astype(jnp.float32) * jax.nn.sigmoid(conv_gate.astype(jnp.float32))
    ).astype(jnp.bfloat16)
    rim_values, rim_ids = shifted(
        (gated_values[local_tokens - rim_width :], doc_ids[local_tokens - rim_width :]), "sp", 1
    )
    padded = jnp.concatenate([rim_values, gated_values], axis=0)
    padded_ids = jnp.concatenate([rim_ids, doc_ids], axis=0)
    kernel = conv_kernel.astype(jnp.float32)
    summed = jnp.zeros((local_tokens, local_width), jnp.float32)
    for tap in range(kernel_taps):
        same_doc = padded_ids[tap : tap + local_tokens] == doc_ids
        summed = summed + jnp.where(
            same_doc[:, None],
            padded[tap : tap + local_tokens].astype(jnp.float32) * kernel[tap][None, :],
            jnp.float32(0.0),
        )
    convolved = summed.astype(jnp.bfloat16)
    group_devices = lax.axis_size("tp")
    total_width = local_width * group_devices
    channel_start = lax.axis_index("tp") * local_width
    activated = normalize_channels(
        convolved, norm_gain_conv, norm_bias_conv, channel_start, total_width
    )
    moved_rows = lax.all_to_all(activated, "tp", split_axis=0, concat_axis=1, tiled=True)
    projected = project_rows(moved_rows, proj_weight)
    state_values = residual.astype(jnp.float32) + projected
    hidden_state = state_values.astype(jnp.bfloat16)
    state_values = hidden_state.astype(jnp.float32)
    normed = (
        state_values
        * lax.rsqrt(jnp.mean(state_values * state_values, axis=1, keepdims=True) + epsilon)
        * norm_gain_moe
    ).astype(jnp.bfloat16)
    group_logits = jnp.dot(normed, group_router, preferred_element_type=jnp.float32)
    expert_logits = jnp.dot(normed, expert_router, preferred_element_type=jnp.float32)
    group_total = group_router.shape[1]
    expert_total = expert_router.shape[1]
    per_group = expert_total // group_total
    first_choice = routing[:, 0]
    second_choice = routing[:, 1]
    chosen_group = first_choice // per_group
    group_exp = jnp.exp(group_logits)
    group_match = chosen_group[:, None] == jnp.arange(group_total, dtype=jnp.int32)[None, :]
    group_prob = jnp.sum(jnp.where(group_match, group_exp, jnp.float32(0.0)), axis=1) / jnp.sum(
        group_exp, axis=1
    )
    expert_iota = jnp.arange(expert_total, dtype=jnp.int32)[None, :]
    first_logit = jnp.sum(
        jnp.where(first_choice[:, None] == expert_iota, expert_logits, jnp.float32(0.0)), axis=1
    )
    second_logit = jnp.sum(
        jnp.where(second_choice[:, None] == expert_iota, expert_logits, jnp.float32(0.0)), axis=1
    )
    first_exp = jnp.exp(first_logit)
    second_exp = jnp.exp(second_logit)
    first_weight = group_prob * first_exp / (first_exp + second_exp)
    second_weight = group_prob * second_exp / (first_exp + second_exp)
    row_count = normed.shape[0]
    capacity = 2 * row_count // expert_total
    flat_experts = routing.reshape(-1)
    indicator = (flat_experts[:, None] == expert_iota).astype(jnp.int32)
    before = jnp.cumsum(indicator, axis=0) - indicator
    position = jnp.sum(before * indicator, axis=1)
    destination = flat_experts * capacity + position
    source = (
        jnp.zeros((2 * row_count,), jnp.int32)
        .at[destination]
        .set(jnp.arange(2 * row_count, dtype=jnp.int32) // 2)
    )
    outgoing = normed[source].reshape(expert_total, capacity, normed.shape[1])
    arrived = lax.all_to_all(outgoing, "sp", split_axis=0, concat_axis=0, tiled=True)
    senders, slot_count, features = arrived.shape
    flattened = arrived.reshape(senders * slot_count, features)
    gate_part = jnp.dot(flattened, expert_gate_w[0], preferred_element_type=jnp.float32)
    up_part = jnp.dot(flattened, expert_up_w[0], preferred_element_type=jnp.float32)
    expert_hidden = (jax.nn.silu(gate_part) * up_part).astype(jnp.bfloat16)
    expert_result = jnp.dot(
        expert_hidden, expert_down_w[0], preferred_element_type=jnp.float32
    ).astype(jnp.bfloat16)
    returned = lax.all_to_all(
        expert_result.reshape(senders, slot_count, features),
        "sp",
        split_axis=0,
        concat_axis=0,
        tiled=True,
    )
    picked = (
        returned.reshape(2 * row_count, normed.shape[1])[destination]
        .reshape(row_count, 2, normed.shape[1])
        .astype(jnp.float32)
    )
    mixture = first_weight[:, None] * picked[:, 0] + second_weight[:, None] * picked[:, 1]
    return (state_values + mixture).astype(jnp.bfloat16)


def solution(mesh):
    placed = (
        P("sp", "tp"),
        P("sp", "tp"),
        P("sp"),
        P(None, "tp"),
        P(),
        P(),
        P("tp", None),
        P(("sp", "tp"), None),
        P(),
        P(),
        P(),
        P(("sp", "tp"), None),
        P("sp", None, None),
        P("sp", None, None),
        P("sp", None, None),
    )
    return jax.shard_map(
        body, mesh=mesh, in_specs=placed, out_specs=P(("sp", "tp"), None), check_vma=False
    )
```

profile of v0, /device:TPU:0, one launch (start us, length us, event | category | flops | bytes accessed | tf_op | source)
XLA Modules:
  0.0 203.7 jit_solution(5720904184012834598)
XLA Ops:
  6.5 0.7 all-gather.2.cloned.1.call-update
  7.3 0.8 slice.297
  8.1 4.9 %collective-permute-start = (s32[30]{0:T(128)S(1)}, s32[30]{0:T(128)S(1)}, u32[]{:S(2)}, u32[]{:S(2)}) collective-permute-start(s32[30]{0:T(128)S(1)} %slice.297), channel_id=1, source_target_pairs={{0,8},{8,16},{16,24},{1,9},{9,17},{17,25},{2,10},{10,18},{18,26},{... | collective-permute-start | bytes 368 | tf_op jit(solution)/shard_map/ppermute | solution.py:12
  13.0 1.8 multiply_convert_fusion.1
  14.8 3.4 %collective-permute-start.1 = (bf16[30,256]{1,0:T(8,128)(2,1)S(1)}, bf16[30,256]{1,0:T(8,128)(2,1)S(1)}, u32[]{:S(2)}, u32[]{:S(2)}) collective-permute-start(bf16[30,256]{1,0:T(8,128)(2,1)S(1)} %slice.402), channel_id=1, source_target_pairs={{0,8},{8,16},{16,24},{1,9},{9,17},{17,25},{2,10},{10,18},{18,26},{... | collective-permute-start | bytes 46088 | tf_op jit(solution)/shard_map/ppermute | solution.py:12
  18.7 0.8 dynamic_slice.6
  19.5 0.8 dynamic_slice.7
  20.8 16.6 %convert_reduce_fusion = (f32[1536]{0:T(1024)S(1)}, f32[1536]{0:T(1024)S(1)}, bf16[1536,256]{1,0:T(8,128)(2,1)}) fusion(f32[256]{0:T(256)S(1)} %bitcast.121, bf16[1536,256]{1,0:T(8,128)(2,1)S(1)} %multiply_convert_fusion.1, f32[256]{0:T(256)S(1)} %bitcast.120, bf16[30,256]{1,0:T(8,128)(2,1)S(1)} %collective-permute-done.1, ...), kind=kLoop, calls=%fused_computation.38 | loop fusion | flops 85324800 | bytes 1678336 | tf_op jit(solution)/shard_map/reduce_sum | solution.py:19
  37.4 30.5 %all-reduce = (f32[1536]{0:T(1024)S(1)}, f32[1536]{0:T(1024)S(1)}) all-reduce(f32[1536]{0:T(1024)S(1)} %get-tuple-element.6, f32[1536]{0:T(1024)S(1)} %get-tuple-element.5), channel_id=1, replica_groups=mesh['sp'=4,'tp'=8] {'tp'}, use_global_device_ids=true, to_apply=%region_3.4 | all-reduce | flops 3072 | bytes 24576 | tf_op jit(solution)/shard_map/psum | solution.py:18
  67.9 2.6 %fusion.15 = bf16[1536,256]{1,0:T(8,128)(2,1)} fusion(bf16[1536,256]{1,0:T(8,128)(2,1)} %get-tuple-element.15, f32[256]{0:T(256)S(1)} %dynamic_slice.7, f32[256]{0:T(256)S(1)} %dynamic_slice.6, f32[1536]{0:T(1024)S(1)} %get-tuple-element.80, f32[1536]{0:T(1024)S(1)} %get-tuple-element.79), kind=kLoop, calls=%fused_computation.52 | loop fusion | flops 3932160 | bytes 1587200 | tf_op jit(solution)/shard_map/convert_element_type | solution.py:26
  70.5 3.6 %all-to-all-start = ((bf16[8,192,256]{2,1,0:T(8,128)(2,1)}), bf16[8,192,256]{2,1,0:T(8,128)(2,1)S(1)}, u32[]{:S(2)}, u32[]{:S(2)}) async-start(bf16[8,192,256]{2,1,0:T(8,128)(2,1)} %bitcast.31), calls=%async_computation | async-start | bytes 1572864 | tf_op jit(solution)/shard_map/all_to_all | solution.py:81
  74.1 1.2 reduce-window.6
  75.3 0.2 slice_reduce_fusion
  76.1 2.9 %scatter_custom_fusion = s32[384]{0:T(512)S(1)} fusion(s32[384]{0:T(512)S(1)} %fusion.132, s32[384]{0:T(512)S(1)} %add_select_fusion, s32[]{:T(128)} %constant.56.clone.1), kind=kCustom, calls=%fused_computation.232 | custom fusion | bytes 1540 | tf_op jit(solution)/shard_map/scatter | solution.py:125
  79.1 30.2 %all-to-all-done = bf16[8,192,256]{2,1,0:T(8,128)(2,1)S(1)} async-done(((bf16[8,192,256]{2,1,0:T(8,128)(2,1)}), bf16[8,192,256]{2,1,0:T(8,128)(2,1)S(1)}, u32[]{:S(2)}, u32[]{:S(2)}) %all-to-all-start) | async-done | bytes 786464 | tf_op jit(solution)/shard_map/all_to_all | solution.py:81
  109.3 1.0 copy.30
  110.2 0.2 all-gather.2.cloned.1.call-done
  110.5 5.7 %multiply_reduce_fusion = (f32[192]{0:T(256)S(1)}, f32[192,2048]{1,0:T(8,128)S(1)}) fusion(bf16[192,2048]{1,0:T(8,128)(2,1)} %bitcast.105, bf16[2048,2048]{1,0:T(8,128)(2,1)} %all-gather.2.cloned.1.call-done, bf16[192,2048]{1,0:T(8,128)(2,1)} %param.22), kind=kOutput, calls=%fused_computation.62 | convolution fusion | flops 1612971776 | bytes 11535104 | tf_op jit(solution)/shard_map/dot_general | solution.py:30
  116.2 1.1 copy-done.1
  117.5 3.1 %gather_fusion = bf16[384,2048]{1,0:T(8,128)(2,1)} fusion(bf16[192,2048]{1,0:T(8,128)(2,1)S(1)} %multiply_convert_fusion, s32[1024]{0:T(1024)S(1)} %pad_clamp_fusion.1), kind=kCustom, calls=%fused_computation | custom fusion | bytes 3147264 | tf_op jit(solution)/shard_map/gather | solution.py:127
  120.7 24.6 %all_to_all.29 = bf16[4,96,2048]{2,1,0:T(8,128)(2,1)S(1)} all-to-all(bf16[4,96,2048]{2,1,0:T(8,128)(2,1)} %bitcast.100), channel_id=1, replica_groups=mesh['sp'=4,'tp'=8] {'sp'}, dimensions={0} | all-to-all | bytes 3145728 | tf_op jit(solution)/shard_map/all_to_all | solution.py:128
  145.3 1.2 copy-done.3
  146.5 1.9 fusion.5
  148.3 5.3 %convolution_convert_fusion = bf16[384,2048]{1,0:T(8,128)(2,1)} fusion(bf16[1,512,2048]{2,1,0:T(8,128)(2,1)S(1)} %copy-done, bf16[384,2048]{1,0:T(8,128)(2,1)} %bitcast.104, bf16[1,2048,512]{2,1,0:T(8,128)(2,1)} %param.28, f32[384,512]{1,0:T(8,128)} %fusion.5), kind=kOutput, calls=%fused_computation.32 | convolution fusion | flops 1612578816 | bytes 8126464 | tf_op jit(solution)/shard_map/dot_general | solution.py:134
  153.6 4.5 %all-to-all-start.2 = ((bf16[4,96,2048]{2,1,0:T(8,128)(2,1)}), bf16[4,96,2048]{2,1,0:T(8,128)(2,1)}, u32[]{:S(2)}, u32[]{:S(2)}) async-start(bf16[4,96,2048]{2,1,0:T(8,128)(2,1)} %bitcast.102), calls=%async_computation.2 | async-start | bytes 3145728 | tf_op jit(solution)/shard_map/all_to_all | solution.py:137
  158.1 0.3 fusion.136
  158.5 0.3 select_reduce_fusion.1
  158.9 17.8 %all-to-all-done.2 = bf16[4,96,2048]{2,1,0:T(8,128)(2,1)} async-done(((bf16[4,96,2048]{2,1,0:T(8,128)(2,1)}), bf16[4,96,2048]{2,1,0:T(8,128)(2,1)}, u32[]{:S(2)}, u32[]{:S(2)}) %all-to-all-start.2) | async-done | bytes 1572896 | tf_op jit(solution)/shard_map/all_to_all | solution.py:137
  176.7 6.7 %gather_fusion.1 = bf16[384,2048]{1,0:T(8,128)(2,1)} fusion(bf16[384,2048]{1,0:T(8,128)(2,1)} %bitcast.43, s32[1024]{0:T(1024)S(1)} %pad_clamp_fusion), kind=kCustom, calls=%fused_computation.1 | custom fusion | bytes 3147264 | tf_op jit(solution)/shard_map/gather | solution.py:145
  183.4 4.7 %reshape.136 = f32[192,2,2048]{2,1,0:T(2,128)} reshape(bf16[384,2048]{1,0:T(8,128)(2,1)} %gather_fusion.1) | data formatting | bytes 4718592 | tf_op jit(solution)/shard_map/convert_element_type | solution.py:147
  188.1 6.2 %fusion.137 = (f32[192,1,2048]{2,1,0:T(1,128)S(1)}, f32[192,1,2048]{2,1,0:T(1,128)S(1)}) fusion(f32[192,2,2048]{2,1,0:T(2,128)} %reshape.136), kind=kLoop, calls=%fused_computation.239 | loop fusion | bytes 6291456 | tf_op jit(solution)/shard_map/slice | solution.py:149
  194.3 2.6 %fusion.20 = bf16[192,2048]{1,0:T(8,128)(2,1)} fusion(f32[192,2048]{1,0:T(8,128)S(1)} %copy-done.2, f32[192,1,2048]{2,1,0:T(1,128)S(1)} %get-tuple-element.17, f32[192,1,2048]{2,1,0:T(1,128)S(1)} %get-tuple-element.16, f32[192]{0:T(256)S(1)} %multiply_divide_fusion, f32[192]{0:T(256)S(1)} %get-tuple-element.13), kind=kLoop, calls=%fused_computation.58 | loop fusion | flops 1966080 | bytes 5506560 | tf_op jit(solution)/shard_map/convert_element_type | solution.py:150
  (52 shorter events, 1.8 us)
Async XLA Ops:
  6.5 141.8 %copy-start = (bf16[1,512,2048]{2,1,0:T(8,128)(2,1)S(1)}, bf16[1,512,2048]{2,1,0:T(8,128)(2,1)}, u32[]{:S(2)}) copy-start(bf16[1,512,2048]{2,1,0:T(8,128)(2,1)} %param.29) | copy-start | bytes 6291460
  6.5 11.7 %copy-start.6 = (s32[192,2]{0,1:T(2,128)S(1)}, s32[192,2]{0,1:T(2,128)}, u32[]{:S(2)}) copy-start(s32[192,2]{0,1:T(2,128)} %param.26) | copy-start | bytes 4612
  6.5 104.0 %all-gather.2.cloned.1.call-start = ((), (), s32[]{:S(2)}) async-start(), calls=%async_computation.3 | async-start | bytes 9437184 | tf_op jit(solution)/shard_map/all_gather | solution.py:32
  7.3 12.2 %copy-start.5 = (bf16[31,256]{1,0:T(8,128)(2,1)S(1)}, bf16[31,256]{1,0:T(8,128)(2,1)}, u32[]{:S(2)}) copy-start(bf16[31,256]{1,0:T(8,128)(2,1)} %param.18) | copy-start | bytes 47620
  7.3 13.0 %copy-start.4 = (s32[1536]{0:T(1024)S(1)}, s32[1536]{0:T(1024)}, u32[]{:S(2)}) copy-start(s32[1536]{0:T(1024)} %param.17) | copy-start | bytes 18436
  8.1 12.2 %collective-permute-start = (s32[30]{0:T(128)S(1)}, s32[30]{0:T(128)S(1)}, u32[]{:S(2)}, u32[]{:S(2)}) collective-permute-start(s32[30]{0:T(128)S(1)} %slice.297), channel_id=1, source_target_pairs={{0,8},{8,16},{16,24},{1,9},{9,17},{17,25},{2,10},{10,18},{18,26},{... | collective-permute-start | bytes 368 | tf_op jit(solution)/shard_map/ppermute | solution.py:12
  14.8 5.9 %collective-permute-start.1 = (bf16[30,256]{1,0:T(8,128)(2,1)S(1)}, bf16[30,256]{1,0:T(8,128)(2,1)S(1)}, u32[]{:S(2)}, u32[]{:S(2)}) collective-permute-start(bf16[30,256]{1,0:T(8,128)(2,1)S(1)} %slice.402), channel_id=1, source_target_pairs={{0,8},{8,16},{16,24},{1,9},{9,17},{17,25},{2,10},{10,18},{18,26},{... | collective-permute-start | bytes 46088 | tf_op jit(solution)/shard_map/ppermute | solution.py:12
  70.5 38.8 %all-to-all-start = ((bf16[8,192,256]{2,1,0:T(8,128)(2,1)}), bf16[8,192,256]{2,1,0:T(8,128)(2,1)S(1)}, u32[]{:S(2)}, u32[]{:S(2)}) async-start(bf16[8,192,256]{2,1,0:T(8,128)(2,1)} %bitcast.31), calls=%async_computation | async-start | bytes 1572864 | tf_op jit(solution)/shard_map/all_to_all | solution.py:81
  110.5 6.9 %copy-start.8 = (f32[2048]{0:T(1024)S(1)}, f32[2048]{0:T(1024)}, u32[]{:S(2)}) copy-start(f32[2048]{0:T(1024)} %param.23) | copy-start | bytes 24580
  116.2 1.1 copy-start.1
  120.7 25.8 %copy-start.10 = (bf16[1,2048,512]{2,1,0:T(8,128)(2,1)S(1)}, bf16[1,2048,512]{2,1,0:T(8,128)(2,1)}, u32[]{:S(2)}) copy-start(bf16[1,2048,512]{2,1,0:T(8,128)(2,1)} %param.27) | copy-start | bytes 6291460
  145.3 1.2 copy-start.3
  153.6 4.5 %copy-start.9 = (bf16[2048,2]{0,1:T(2,128)(2,1)S(1)}, bf16[2048,2]{0,1:T(2,128)(2,1)}, u32[]{:S(2)}) copy-start(bf16[2048,2]{0,1:T(2,128)(2,1)} %param.24) | copy-start | bytes 24580
  153.6 4.9 %copy-start.7 = (bf16[2048,4]{0,1:T(4,128)(2,1)S(1)}, bf16[2048,4]{0,1:T(4,128)(2,1)}, u32[]{:S(2)}) copy-start(bf16[2048,4]{0,1:T(4,128)(2,1)} %param.25) | copy-start | bytes 49156
  153.6 23.1 %all-to-all-start.2 = ((bf16[4,96,2048]{2,1,0:T(8,128)(2,1)}), bf16[4,96,2048]{2,1,0:T(8,128)(2,1)}, u32[]{:S(2)}, u32[]{:S(2)}) async-start(bf16[4,96,2048]{2,1,0:T(8,128)(2,1)} %bitcast.102), calls=%async_computation.2 | async-start | bytes 3145728 | tf_op jit(solution)/shard_map/all_to_all | solution.py:137
  188.1 6.2 %copy-start.2 = (f32[192,2048]{1,0:T(8,128)S(1)}, f32[192,2048]{1,0:T(8,128)}, u32[]{:S(2)}) copy-start(f32[192,2048]{1,0:T(8,128)} %copy-done.1) | copy-start | bytes 4718596
Sparse Core Ops, SparseCore 0:
  8.9 101.5 all-gather.1
where the time goes:
time: 204 us
  blocking collectives  55.1 us (27%)
  waiting for transfers between devices  49 us (24%)
  local copies, waits for them, and re-layouts  30.2 us (15%)
  other arithmetic  25.9 us (13%)
  starting transfers between devices  16.3 us (8%)
  between operations  13.7 us (7%)
  matrix products  13.5 us (7%)
    psum x1, blocking collectives, normalize_channels(): lax.psum((jnp.sum(values, axis=1), jnp.sum(values * values, axis=1)), 'tp')  30.5 us
    all_to_all x1, waiting for transfers between devices, body(): lax.all_to_all(activated, 'tp', split_axis=0, concat_axis=1, tiled=True)  30.2 us
    all_to_all x1, blocking collectives, body(): lax.all_to_all(outgoing, 'sp', split_axis=0, concat_axis=0, tiled=True)  24.6 us
    all_to_all x1, waiting for transfers between devices, body(): lax.all_to_all(expert_result.reshape(senders, slot_count, features), 'sp'...  17.8 us
    reduce_sum x1, other arithmetic, normalize_channels(): jnp.sum(values, axis=1)  16.6 us
    ppermute x2, starting transfers between devices, shifted(): return lax.ppermute(array, axis, pairs)  8.26 us
    gather x1, local copies, waits for them, and re-layouts, body(): returned.reshape(2 * row_count, normed.shape[1])[destination]  6.68 us
    slice x1, local copies, waits for them, and re-layouts, body(): picked[:, 0]  6.18 us
  transfers between devices with their start and end apart: 5, of which 3 were waited for; matrix products, arithmetic and copies ran while one was open for 15% of the time, Pallas kernels for 0%

commit v1 on v0

v1 whole, which is shorter than its diff:
```python
import jax
import jax.numpy as jnp
from jax import lax
from jax.sharding import PartitionSpec as P

epsilon = 1e-06


def halo(gated_values, doc_ids, rim_width):
    local_tokens, local_width = gated_values.shape
    last_id = doc_ids[local_tokens - 1]
    same = doc_ids[local_tokens - rim_width :] == last_id
    rim = jnp.where(same[:, None], gated_values[local_tokens - rim_width :], jnp.bfloat16(0.0))
    id_row = jnp.full((1, local_width), last_id.astype(jnp.bfloat16))
    count = lax.axis_size("sp")
    pairs = [(i, i + 1) for i in range(count - 1)]
    return lax.ppermute(jnp.concatenate([rim, id_row], axis=0), "sp", pairs)


def body(
    conv_value,
    conv_gate,
    doc_ids,
    conv_kernel,
    norm_gain_conv,
    norm_bias_conv,
    proj_weight,
    residual,
    norm_gain_moe,
    group_router,
    expert_router,
    routing,
    expert_gate_w,
    expert_up_w,
    expert_down_w,
):
    local_tokens, local_width = conv_value.shape
    kernel_taps = conv_kernel.shape[0]
    rim_width = kernel_taps - 1
    sp_size = lax.axis_size("sp")
    tp_size = lax.axis_size("tp")
    weight_rows = proj_weight.shape[0] // sp_size
    weight_piece = lax.dynamic_slice_in_dim(
        proj_weight, lax.axis_index("sp") * weight_rows, weight_rows
    )
    weight_full = lax.all_gather(weight_piece, ("sp", "tp"), axis=0, tiled=True)
    gated_values = (
        conv_value.astype(jnp.float32) * jax.nn.sigmoid(conv_gate.astype(jnp.float32))
    ).astype(jnp.bfloat16)
    arrived_rim = halo(gated_values, doc_ids, rim_width)
    rim_id = arrived_rim[rim_width, 0].astype(jnp.int32)
    padded = jnp.concatenate([arrived_rim[:rim_width], gated_values], axis=0)
    padded_ids = jnp.concatenate([jnp.full((rim_width,), rim_id), doc_ids], axis=0)
    kernel = conv_kernel.astype(jnp.float32)
    summed = jnp.zeros((local_tokens, local_width), jnp.float32)
    for tap in range(kernel_taps):
        same_doc = padded_ids[tap : tap + local_tokens] == doc_ids
        summed = summed + jnp.where(
            same_doc[:, None],
            padded[tap : tap + local_tokens].astype(jnp.float32) * kernel[tap][None, :],
            jnp.float32(0.0),
        )
    convolved = summed.astype(jnp.bfloat16)
    values = lax.all_to_all(convolved, "tp", split_axis=0, concat_axis=1, tiled=True).astype(
        jnp.float32
    )
    average = jnp.mean(values, axis=1, keepdims=True)
    centered = values - average
    variance = jnp.mean(centered * centered, axis=1, keepdims=True)
    activated = jax.nn.silu(
        centered * lax.rsqrt(variance + epsilon) * norm_gain_conv + norm_bias_conv
    ).astype(jnp.bfloat16)
    rows, channels = activated.shape
    reordered = (
        activated.reshape(rows, tp_size, sp_size, weight_rows)
        .transpose(0, 2, 1, 3)
        .reshape(rows, channels)
    )
    projected = jnp.dot(reordered, weight_full, preferred_element_type=jnp.float32)
    hidden_state = (residual.astype(jnp.float32) + projected).astype(jnp.bfloat16)
    state_values = hidden_state.astype(jnp.float32)
    normed = (
        state_values
        * lax.rsqrt(jnp.mean(state_values * state_values, axis=1, keepdims=True) + epsilon)
        * norm_gain_moe
    ).astype(jnp.bfloat16)
    group_total = group_router.shape[1]
    expert_total = expert_router.shape[1]
    per_group = expert_total // group_total
    capacity = 2 * rows // expert_total
    expert_iota = jnp.arange(expert_total, dtype=jnp.int32)[None, :]
    chosen = (routing[:, 0:1] == expert_iota) | (routing[:, 1:2] == expert_iota)
    chosen_group = (routing[:, 0:1] // per_group) == jnp.arange(group_total, dtype=jnp.int32)[
        None, :
    ]
    row_iota = jnp.arange(rows, dtype=jnp.int32)
    earlier = (row_iota[None, :] < row_iota[:, None]).astype(jnp.bfloat16)
    before = jnp.dot(earlier, chosen.astype(jnp.bfloat16), preferred_element_type=jnp.float32)
    slot = jnp.where(chosen, before, jnp.float32(-1.0))
    slot_iota = jnp.arange(capacity, dtype=jnp.int32).astype(jnp.float32)
    picks = (slot.T[:, None, :] == slot_iota[None, :, None]).astype(jnp.bfloat16)
    outgoing = (
        jnp.dot(
            picks.reshape(expert_total * capacity, rows),
            normed,
            preferred_element_type=jnp.float32,
        )
        .astype(jnp.bfloat16)
        .reshape(sp_size, -1, capacity, channels)
    )
    arrived = lax.all_to_all(outgoing, "sp", split_axis=0, concat_axis=0, tiled=True)
    group_logits = jnp.dot(normed, group_router, preferred_element_type=jnp.float32)
    expert_logits = jnp.dot(normed, expert_router, preferred_element_type=jnp.float32)
    group_exp = jnp.exp(group_logits)
    group_prob = jnp.sum(
        jnp.where(chosen_group, group_exp, jnp.float32(0.0)), axis=1, keepdims=True
    ) / jnp.sum(group_exp, axis=1, keepdims=True)
    chosen_exp = jnp.where(chosen, jnp.exp(expert_logits), jnp.float32(0.0))
    mix_weight = group_prob * chosen_exp / jnp.sum(chosen_exp, axis=1, keepdims=True)
    flattened = arrived.reshape(-1, channels)
    gate_part = jnp.dot(flattened, expert_gate_w[0], preferred_element_type=jnp.float32)
    up_part = jnp.dot(flattened, expert_up_w[0], preferred_element_type=jnp.float32)
    expert_hidden = (jax.nn.silu(gate_part) * up_part).astype(jnp.bfloat16)
    expert_result = jnp.dot(
        expert_hidden, expert_down_w[0], preferred_element_type=jnp.float32
    ).astype(jnp.bfloat16)
    returned = lax.all_to_all(
        expert_result.reshape(sp_size, -1, channels),
        "sp",
        split_axis=0,
        concat_axis=0,
        tiled=True,
    ).reshape(expert_total * capacity, channels)
    spread = jnp.where(
        slot[:, :, None] == slot_iota[None, None, :], mix_weight[:, :, None], jnp.float32(0.0)
    )
    mixture = jnp.dot(
        spread.astype(jnp.bfloat16).reshape(rows, expert_total * capacity),
        returned,
        preferred_element_type=jnp.float32,
    )
    return (state_values + mixture).astype(jnp.bfloat16)


def solution(mesh):
    placed = (
        P("sp", "tp"),
        P("sp", "tp"),
        P("sp"),
        P(None, "tp"),
        P(),
        P(),
        P("tp", None),
        P(("sp", "tp"), None),
        P(),
        P(),
        P(),
        P(("sp", "tp"), None),
        P("sp", None, None),
        P("sp", None, None),
        P("sp", None, None),
    )
    return jax.shard_map(
        body, mesh=mesh, in_specs=placed, out_specs=P(("sp", "tp"), None), check_vma=False
    )
```

time: 204 us -> 170 us (0.83)
  blocking collectives: 55.1 us -> 23 us
  local copies, waits for them, and re-layouts: 30.2 us -> 8.38 us
  waiting for transfers between devices: 49 us -> 68.7 us
  matrix products: 13.5 us -> 17.6 us
  other arithmetic: 25.9 us -> 22.7 us
  starting transfers between devices: 16.3 us -> 14.2 us
    psum x1 -> x0, blocking collectives: 30.5 us -> none  [normalize_channels(): lax.psum((jnp.sum(values, axis=1), jnp.sum(values * values, axis=1)), 'tp')]
    all_gather x1, waiting for transfers between devices: 0.25 us -> 20.5 us  [body(): weight_full = lax.all_gather(weight_piece, ('sp', 'tp'), axis=0, tiled=True)]
    reduce_sum x2, other arithmetic: 16.6 us -> 0.54 us  [the longest x1 0.36 us: body(): variance = jnp.mean(centered * centered, axis=1, keepdims=True)]
    convert_element_type x3, other arithmetic: 5.21 us -> 16 us  [the longest x1 14.7 us: body(): convolved = summed.astype(jnp.bfloat16)]
    gather x2 -> x0, local copies, waits for them, and re-layouts: 9.81 us -> none  [the longest x1 6.68 us: body(): returned.reshape(2 * row_count, normed.shape[1])[destination]]
    slice x4 -> x2, local copies, waits for them, and re-layouts: 7.23 us -> 1.79 us  [the longest x1 1.27 us: halo(): last_id = doc_ids[local_tokens - 1]]
    dot_general x1 -> x4, matrix products: 5.7 us -> 9.74 us  [the longest x1 5.46 us: body(): jnp.dot(reordered, weight_full, preferred_element_type=jnp.float32)]
    ppermute x2 -> x1, starting transfers between devices: 8.26 us -> 4.87 us  [halo(): return lax.ppermute(jnp.concatenate([rim, id_row], axis=0), 'sp', pairs)]
  transfers between devices with their start and end apart: 5 -> 4, of which waited for: 3 -> 4; matrix products, arithmetic and copies ran while one was open for 15% -> 17% of each run, Pallas kernels for 0% -> 0%
where the time goes in v1:
time: 170 us; the launch traced here: 169 us
  waiting for transfers between devices  68.7 us (40%)
  blocking collectives  23 us (14%)
  other arithmetic  22.7 us (13%)
  matrix products  17.6 us (10%)
  between operations  14.9 us (9%)
  starting transfers between devices  14.2 us (8%)
  local copies, waits for them, and re-layouts  8.38 us (5%)
    all_to_all x1, waiting for transfers between devices, body(): lax.all_to_all(convolved, 'tp', split_axis=0, concat_axis=1, tiled=True)  28.8 us
    all_to_all x1, blocking collectives, body(): lax.all_to_all(outgoing, 'sp', split_axis=0, concat_axis=0, tiled=True)  23 us
    all_gather x1, waiting for transfers between devices, body(): weight_full = lax.all_gather(weight_piece, ('sp', 'tp'), axis=0, tiled=True)  20.5 us
    all_to_all x1, waiting for transfers between devices, body(): lax.all_to_all(expert_result.reshape(sp_size, -1, channels), 'sp', split_...  18 us
    convert_element_type x1, other arithmetic, body(): convolved = summed.astype(jnp.bfloat16)  14.7 us
    dot_general x1, matrix products, body(): jnp.dot(reordered, weight_full, preferred_element_type=jnp.float32)  5.46 us
    dot_general x1, matrix products, body(): jnp.dot(expert_hidden, expert_down_w[0], preferred_element_type=jnp.float32)  5.31 us
    all_to_all x1, starting transfers between devices, body(): lax.all_to_all(convolved, 'tp', split_axis=0, concat_axis=1, tiled=True)  4.88 us
  transfers between devices with their start and end apart: 4, of which 4 were waited for; matrix products, arithmetic and copies ran while one was open for 17% of the time, Pallas kernels for 0%

profile of v1, /device:TPU:0, one launch (start us, length us, event | category | flops | bytes accessed | tf_op | source)
XLA Modules:
  0.0 169.5 jit_solution(4503496915675221949)
XLA Ops:
  6.5 1.8 %constant_dynamic-slice_fusion = bf16[64,2048]{1,0:T(8,128)(2,1)} fusion(bf16[256,2048]{1,0:T(8,128)(2,1)} %param.21, s32[]{:T(128)S(6)} %select_n.153), kind=kLoop, calls=%fused_computation.157 | loop fusion | bytes 524292 | tf_op jit(solution)/shard_map/dynamic_slice | solution.py:43
  8.4 1.3 slice.296
  10.3 1.4 slice_compare_fusion.30
  11.7 1.8 %multiply_convert_fusion.2 = bf16[1536,256]{1,0:T(8,128)(2,1)S(1)} fusion(bf16[1536,256]{1,0:T(8,128)(2,1)} %param.16, bf16[1536,256]{1,0:T(8,128)(2,1)} %param.15), kind=kLoop, calls=%fused_computation.51 | loop fusion | flops 2752512 | bytes 2359296 | tf_op jit(solution)/shard_map/convert_element_type | solution.py:49
  13.7 4.9 %collective-permute-start = (bf16[31,256]{1,0:T(8,128)(2,1)S(1)}, bf16[31,256]{1,0:T(8,128)(2,1)S(1)}, u32[]{:S(2)}, u32[]{:S(2)}) collective-permute-start(bf16[31,256]{1,0:T(8,128)(2,1)S(1)} %concatenate.9), channel_id=1, source_target_pairs={{0,8},{8,16},{16,24},{1,9},{9,17},{17,25},{2,10},{10,18},{18,26},{... | collective-permute-start | bytes 47624 | tf_op jit(solution)/shard_map/ppermute | solution.py:17
  18.6 1.4 collective-permute-done
  20.0 0.5 slice.394
  21.6 14.7 %add_convert_fusion = bf16[1536,256]{1,0:T(8,128)(2,1)} fusion(bf16[1536,256]{1,0:T(8,128)(2,1)S(1)} %multiply_convert_fusion.2, bf16[30,256]{1,0:T(8,128)(2,1)S(1)} %bitcast.93, f32[256]{0:T(256)S(1)} %bitcast.131, f32[256]{0:T(256)S(1)} %bitcast.130, f32[256]{0:T(256)S(1)} %bitcast.129, f32[256]{0:T(256)S(1)} %bitcast.128, f32[256]{0:T(256)S(1)} %bitcast.127, ...), kind=kLoop, calls=%fused_computation.50 | loop fusion | flops 83755008 | bytes 1666048 | tf_op jit(solution)/shard_map/convert_element_type | solution.py:63
  36.2 4.9 %all-to-all-start = ((bf16[8,192,256]{2,1,0:T(8,128)(2,1)}), bf16[8,192,256]{2,1,0:T(8,128)(2,1)S(1)}, u32[]{:S(2)}, u32[]{:S(2)}) async-start(bf16[8,192,256]{2,1,0:T(8,128)(2,1)} %bitcast.89), calls=%async_computation | async-start | bytes 1572864 | tf_op jit(solution)/shard_map/all_to_all | solution.py:64
  41.4 0.1 bitcast_select_fusion
  41.5 0.1 bitcast_compare_fusion
  41.7 28.8 %all-to-all-done = bf16[8,192,256]{2,1,0:T(8,128)(2,1)S(1)} async-done(((bf16[8,192,256]{2,1,0:T(8,128)(2,1)}), bf16[8,192,256]{2,1,0:T(8,128)(2,1)S(1)}, u32[]{:S(2)}, u32[]{:S(2)}) %all-to-all-start) | async-done | bytes 786464 | tf_op jit(solution)/shard_map/all_to_all | solution.py:64
  70.5 1.3 convert_bitcast_fusion
  71.8 2.8 %copy.19 = f32[192,8,256]{0,2,1:T(8,128)} copy(f32[192,8,256]{2,0,1:T(8,128)} %convert_bitcast_fusion) | data formatting | bytes 3145728 | tf_op jit(solution)/shard_map/convert_element_type | solution.py:64
  74.6 0.2 convert_reduce_fusion
  74.8 0.4 fusion.10
  75.2 2.1 %fusion.18 = bf16[192,4,8,64]{0,3,1,2:T(8,128)(2,1)S(1)} fusion(f32[8,4,64]{2,1,0:T(4,128)S(1)} %add.175, f32[8,4,64]{2,1,0:T(4,128)S(1)} %mul.477, f32[192]{0:T(256)S(1)} %add_rsqrt_fusion.1, f32[192,8,4,64]{0,3,2,1:T(8,128)} %bitcast.86, f32[192]{0:T(256)S(1)} %broadcast_multiply_fusion), kind=kLoop, calls=%fused_computation.57 | loop fusion | flops 3538944 | bytes 2377216 | tf_op jit(solution)/shard_map/transpose | solution.py:76
  77.3 0.1 copy.20
  77.4 20.5 %all-gather.2.cloned.1.call-done = bf16[2048,2048]{1,0:T(8,128)(2,1)} async-done(((bf16[64,2048]{1,0:T(8,128)(2,1)}), bf16[2048,2048]{1,0:T(8,128)(2,1)}) %all-gather.2.cloned.1.call-update) | async-done | bytes 8388624 | tf_op jit(solution)/shard_map/all_gather | solution.py:46
  97.9 5.5 %multiply_reduce_fusion = (f32[192]{0:T(256)S(1)}, f32[192,2048]{1,0:T(8,128)S(1)}) fusion(bf16[192,2048]{0,1:T(8,128)(2,1)S(1)} %bitcast.88, bf16[2048,2048]{1,0:T(8,128)(2,1)} %all-gather.2.cloned.1.call-done, bf16[192,2048]{1,0:T(8,128)(2,1)} %param.22), kind=kOutput, calls=%fused_computation.49 | convolution fusion | flops 1612971776 | bytes 11535104 | tf_op jit(solution)/shard_map/dot_general | solution.py:79
  103.4 0.2 multiply_convert_fusion.1
  103.6 0.6 convolution_convert_fusion.1
  104.2 0.4 copy-done.1
  104.5 23.0 %all_to_all.23 = bf16[4,1,96,2048]{3,2,1,0:T(8,128)(2,1)S(1)} all-to-all(bf16[4,1,96,2048]{3,2,1,0:T(8,128)(2,1)S(1)} %bitcast.87), channel_id=1, replica_groups=mesh['sp'=4,'tp'=8] {'sp'}, dimensions={0} | all-to-all | bytes 3145728 | tf_op jit(solution)/shard_map/all_to_all | solution.py:111
  127.5 1.1 copy-done.2
  128.7 1.9 %fusion.7 = f32[384,512]{1,0:T(8,128)} fusion(bf16[384,2048]{1,0:T(8,128)(2,1)S(1)} %bitcast.91, bf16[1,2048,512]{2,1,0:T(8,128)(2,1)S(1)} %copy-done.11), kind=kOutput, calls=%fused_computation.43 | convolution fusion | flops 805306368 | bytes 4456448 | tf_op jit(solution)/shard_map/dot_general | solution.py:121
  130.6 5.3 %convolution_convert_fusion = bf16[384,2048]{1,0:T(8,128)(2,1)} fusion(bf16[1,512,2048]{2,1,0:T(8,128)(2,1)S(1)} %copy-done, bf16[384,2048]{1,0:T(8,128)(2,1)} %bitcast.92, bf16[1,2048,512]{2,1,0:T(8,128)(2,1)} %param.28, f32[384,512]{1,0:T(8,128)} %fusion.7), kind=kOutput, calls=%fused_computation.29 | convolution fusion | flops 1612578816 | bytes 8126464 | tf_op jit(solution)/shard_map/dot_general | solution.py:124
  135.9 4.5 %all-to-all-start.2 = ((bf16[4,96,2048]{2,1,0:T(8,128)(2,1)}), bf16[4,96,2048]{2,1,0:T(8,128)(2,1)}, u32[]{:S(2)}, u32[]{:S(2)}) async-start(bf16[4,96,2048]{2,1,0:T(8,128)(2,1)} %bitcast.90), calls=%async_computation.2 | async-start | bytes 3145728 | tf_op jit(solution)/shard_map/all_to_all | solution.py:127
  140.4 0.3 fusion.67
  140.7 0.3 fusion.70
  141.1 18.0 %all-to-all-done.2 = bf16[4,96,2048]{2,1,0:T(8,128)(2,1)} async-done(((bf16[4,96,2048]{2,1,0:T(8,128)(2,1)}), bf16[4,96,2048]{2,1,0:T(8,128)(2,1)}, u32[]{:S(2)}, u32[]{:S(2)}) %all-to-all-start.2) | async-done | bytes 1572896 | tf_op jit(solution)/shard_map/all_to_all | solution.py:127
  159.0 3.6 %fusion.1 = bf16[192,2048]{1,0:T(8,128)(2,1)} fusion(f32[192,2048]{1,0:T(8,128)} %copy-done.1, bf16[4,96,2048]{2,1,0:T(8,128)(2,1)} %all-to-all-done.2, bf16[192,4]{0,1:T(4,128)(2,1)S(1)} %multiply_divide_fusion, f32[96]{0:T(128)S(1)} %iota_convert_fusion, f32[192,4]{0,1:T(4,128)S(1)} %broadcast_select_fusion), kind=kOutput, calls=%fused_computation.34 | convolution fusion | flops 302923776 | bytes 3937152 | tf_op jit(solution)/shard_map/dot_general | solution.py:137
  (44 shorter events, 0.8 us)
Async XLA Ops:
  6.5 124.0 %copy-start = (bf16[1,512,2048]{2,1,0:T(8,128)(2,1)S(1)}, bf16[1,512,2048]{2,1,0:T(8,128)(2,1)}, u32[]{:S(2)}) copy-start(bf16[1,512,2048]{2,1,0:T(8,128)(2,1)} %param.29) | copy-start | bytes 6291460
  6.5 91.4 %all-gather.2.cloned.1.call-start = ((), (), s32[]{:S(2)}) async-start(), calls=%async_computation.3 | async-start | bytes 8650752 | tf_op jit(solution)/shard_map/all_gather | solution.py:46
  6.5 12.0 %copy-start.4 = (bf16[31,256]{1,0:T(8,128)(2,1)S(1)}, bf16[31,256]{1,0:T(8,128)(2,1)}, u32[]{:S(2)}) copy-start(bf16[31,256]{1,0:T(8,128)(2,1)} %param.18) | copy-start | bytes 47620
  6.5 14.6 %copy-start.3 = (s32[1536]{0:T(1024)S(1)}, s32[1536]{0:T(1024)}, u32[]{:S(2)}) copy-start(s32[1536]{0:T(1024)} %param.17) | copy-start | bytes 18436
  13.7 6.3 %collective-permute-start = (bf16[31,256]{1,0:T(8,128)(2,1)S(1)}, bf16[31,256]{1,0:T(8,128)(2,1)S(1)}, u32[]{:S(2)}, u32[]{:S(2)}) collective-permute-start(bf16[31,256]{1,0:T(8,128)(2,1)S(1)} %concatenate.9), channel_id=1, source_target_pairs={{0,8},{8,16},{16,24},{1,9},{9,17},{17,25},{2,10},{10,18},{18,26},{... | collective-permute-start | bytes 47624 | tf_op jit(solution)/shard_map/ppermute | solution.py:17
  21.5 19.6 %copy-start.8 = (f32[2048]{0:T(1024)S(1)}, f32[2048]{0:T(1024)}, u32[]{:S(2)}) copy-start(f32[2048]{0:T(1024)} %param.20) | copy-start | bytes 24580
  21.5 19.7 %copy-start.9 = (f32[2048]{0:T(1024)S(1)}, f32[2048]{0:T(1024)}, u32[]{:S(2)}) copy-start(f32[2048]{0:T(1024)} %param.19) | copy-start | bytes 24580
  21.5 19.8 %copy-start.10 = (s32[192,2]{0,1:T(2,128)S(1)}, s32[192,2]{0,1:T(2,128)}, u32[]{:S(2)}) copy-start(s32[192,2]{0,1:T(2,128)} %param.26) | copy-start | bytes 4612
  36.2 34.3 %all-to-all-start = ((bf16[8,192,256]{2,1,0:T(8,128)(2,1)}), bf16[8,192,256]{2,1,0:T(8,128)(2,1)S(1)}, u32[]{:S(2)}, u32[]{:S(2)}) async-start(bf16[8,192,256]{2,1,0:T(8,128)(2,1)} %bitcast.89), calls=%async_computation | async-start | bytes 1572864 | tf_op jit(solution)/shard_map/all_to_all | solution.py:64
  97.9 5.5 %copy-start.6 = (f32[2048]{0:T(1024)S(1)}, f32[2048]{0:T(1024)}, u32[]{:S(2)}) copy-start(f32[2048]{0:T(1024)} %param.23) | copy-start | bytes 24580
  103.4 1.2 copy-start.1
  104.5 24.2 %copy-start.11 = (bf16[1,2048,512]{2,1,0:T(8,128)(2,1)S(1)}, bf16[1,2048,512]{2,1,0:T(8,128)(2,1)}, u32[]{:S(2)}) copy-start(bf16[1,2048,512]{2,1,0:T(8,128)(2,1)} %param.27) | copy-start | bytes 6291460
  127.5 1.1 copy-start.2
  135.9 4.5 %copy-start.7 = (bf16[2048,2]{0,1:T(2,128)(2,1)S(1)}, bf16[2048,2]{0,1:T(2,128)(2,1)}, u32[]{:S(2)}) copy-start(bf16[2048,2]{0,1:T(2,128)(2,1)} %param.24) | copy-start | bytes 24580
  135.9 4.9 %copy-start.5 = (bf16[2048,4]{0,1:T(4,128)(2,1)S(1)}, bf16[2048,4]{0,1:T(4,128)(2,1)}, u32[]{:S(2)}) copy-start(bf16[2048,4]{0,1:T(4,128)(2,1)} %param.25) | copy-start | bytes 49156
  135.9 23.2 %all-to-all-start.2 = ((bf16[4,96,2048]{2,1,0:T(8,128)(2,1)}), bf16[4,96,2048]{2,1,0:T(8,128)(2,1)}, u32[]{:S(2)}, u32[]{:S(2)}) async-start(bf16[4,96,2048]{2,1,0:T(8,128)(2,1)} %bitcast.90), calls=%async_computation.2 | async-start | bytes 3145728 | tf_op jit(solution)/shard_map/all_to_all | solution.py:127
Sparse Core Ops, SparseCore 0:
  10.3 87.5 all-gather.1

commit v2 on v1

v2 whole, which is shorter than its diff:
```python
import functools

import jax
import jax.numpy as jnp
from jax import lax
from jax.experimental import pallas as pl
from jax.experimental.pallas import tpu as pltpu
from jax.sharding import PartitionSpec as P

epsilon = 1e-06
MESH = pl.DeviceIdType.MESH
F32 = jnp.float32
BF16 = jnp.bfloat16
HALO = 32


def gate(value, gate_value):
    return (value.astype(F32) * jax.nn.sigmoid(gate_value.astype(F32))).astype(BF16)


def kernel(
    S,
    T,
    G,
    value_hbm,
    gate_hbm,
    least_tap_ref,
    rim_keep_ref,
    last_id_ref,
    first_id_ref,
    kernel_ref,
    gain_conv_ref,
    bias_conv_ref,
    weight_hbm,
    residual_hbm,
    gain_moe_ref,
    router_ref,
    routing_ref,
    gate_w_hbm,
    up_w_hbm,
    down_w_hbm,
    out_ref,
    value,
    gates,
    wfull,
    residual,
    gate_w,
    up_w,
    down_w,
    rim_out,
    rim_in,
    padded,
    taps,
    conv_out,
    conv_in,
    act,
    hidden,
    normed,
    outgoing,
    arrived,
    ffn_hidden,
    results,
    returned,
    local_sem,
    wl_sem,
    rim_sem,
    wz_send,
    wz_recv,
    wx_send,
    wx_recv,
    wp_send,
    wp_recv,
    a2a_send,
    a2a_recv,
    disp_send,
    disp_recv,
    ret_send,
    ret_recv,
):
    s = lax.axis_index("sp")
    t = lax.axis_index("tp")
    Z = T // 2
    z = t // 2
    core = t % 2
    partner = 2 * z + 1 - core
    tokens, width = value.shape
    block = tokens // T
    n_taps = kernel_ref.shape[0]
    piece = wfull.shape[3]
    D = S * piece

    def remote(src, dst, send, recv, sp_to, tp_to):
        return pltpu.make_async_remote_copy(
            src_ref=src,
            dst_ref=dst,
            send_sem=send,
            recv_sem=recv,
            device_id=(sp_to, tp_to),
            device_id_type=MESH,
        )

    loads = [
        pltpu.make_async_copy(a, b, local_sem.at[i])
        for i, (a, b) in enumerate(
            [
                (value_hbm, value),
                (gate_hbm, gates),
                (residual_hbm, residual),
                (gate_w_hbm, gate_w),
                (up_w_hbm, up_w),
                (down_w_hbm, down_w),
            ]
        )
    ]
    own_w = [
        pltpu.make_async_copy(
            weight_hbm.at[:, pl.ds(j * piece, piece)], wfull.at[t, j], wl_sem.at[j]
        )
        for j in range(S)
    ]
    loads[0].start()
    loads[1].start()
    for c in own_w:
        c.start()
    for c in loads[2:]:
        c.start()

    barrier = pltpu.get_barrier_semaphore()
    for k in range(1, T):
        pl.semaphore_signal(
            barrier, inc=1, device_id=(s, lax.rem(t + k, T)), device_id_type=MESH
        )
    for k in range(1, S):
        pl.semaphore_signal(
            barrier, inc=1, device_id=(lax.rem(s + k, S), t), device_id_type=MESH
        )
    pl.semaphore_wait(barrier, T + S - 2)

    for c in own_w:
        c.wait()
    waits = []
    for k in range(1, Z):
        to = 2 * lax.rem(z + k, Z) + core
        c = remote(wfull.at[t, s], wfull.at[t, s], wz_send.at[k], wz_recv.at[z], s, to)
        c.start()
        waits.append(c)
    c = remote(wfull.at[t], wfull.at[t], wp_send.at[z], wp_recv.at[z], s, partner)
    c.start()
    waits.append(c)

    loads[0].wait()
    loads[1].wait()
    tail = pl.ds(tokens - HALO, HALO)
    rim = gate(value[tail, :], gates[tail, :]).astype(F32) * rim_keep_ref[...]
    rim_out[0:HALO, :] = rim.astype(BF16)
    rim_out[HALO : HALO + 16, :] = last_id_ref[...]
    rim_copy = remote(
        rim_out, rim_in, rim_sem.at[0], rim_sem.at[1], lax.rem(s + 1, S), t
    )
    rim_copy.start()

    def gate_rows(i, _):
        rows = pl.ds(pl.multiple_of(i * 64, 64), 64)
        to_rows = pl.ds(pl.multiple_of(HALO + i * 64, 32), 64)
        padded[to_rows, :] = gate(value[rows, :], gates[rows, :]).astype(F32)
        return 0

    lax.fori_loop(0, tokens // 64, gate_rows, 0)
    taps[0:n_taps, :] = kernel_ref[...].astype(F32)
    rim_copy.wait()
    same = (rim_in[HALO : HALO + 1, :].astype(F32) == first_id_ref[0:1, :]) & (s > 0)
    padded[0:HALO, :] = jnp.where(same, rim_in[0:HALO, :].astype(F32), jnp.float32(0.0))

    step_rows = 32 if block % 32 == 0 else 8
    lanes = min(width, 128)

    def conv_block(owner):
        def conv_rows(i, _):
            base = pl.multiple_of(owner * block + i * step_rows, 8)
            least = least_tap_ref[pl.ds(base, step_rows), :]
            window = padded[pl.ds(base, step_rows + HALO), :]
            total = jnp.zeros((step_rows, width), F32)
            for tap in range(n_taps):
                at = tap + HALO + 1 - n_taps
                valid = least <= tap
                product = window[at : at + step_rows, :] * taps[tap : tap + 1, :]
                parts = [
                    jnp.where(valid, product[:, j : j + lanes], jnp.float32(0.0))
                    for j in range(0, width, lanes)
                ]
                total = total + jnp.concatenate(parts, axis=1)
            conv_out[
                owner, pl.ds(pl.multiple_of(i * step_rows, step_rows), step_rows), :
            ] = total.astype(BF16)
            return 0

        lax.fori_loop(0, block // step_rows, conv_rows, 0)

    def conv_send(k, _):
        owner = lax.rem(t + k, T)
        conv_block(owner)
        remote(
            conv_out.at[owner],
            conv_in.at[t],
            a2a_send.at[owner],
            a2a_recv.at[t],
            s,
            owner,
        ).start()
        return 0

    lax.fori_loop(1, T, conv_send, 0)
    conv_block(t)
    conv_in[t, :, :] = conv_out[t, :, :]

    for k in range(1, Z):
        from_z = lax.rem(z - k + Z, Z)
        row = 2 * from_z + core
        remote(
            wfull.at[row, s], wfull.at[row, s], wz_send.at[k], wz_recv.at[from_z], s, t
        ).wait_recv()
        for j in range(1, S):
            c = remote(
                wfull.at[row, s],
                wfull.at[row, s],
                wx_send.at[j, from_z],
                wx_recv.at[s, from_z],
                lax.rem(s + j, S),
                t,
            )
            c.start()
            waits.append(c)

    rows = block
    E = S
    cap = 2 * rows // E
    lane = lax.broadcasted_iota(jnp.int32, (rows, 128), 1)
    first = routing_ref[:, 0:1]
    second = routing_ref[:, 1:2]
    chosen = (lane == first + G) | (lane == second + G)
    in_group = lane == first // (E // G)
    tri = lax.broadcasted_iota(jnp.int32, (rows, rows), 0) > lax.broadcasted_iota(
        jnp.int32, (rows, rows), 1
    )
    before = jnp.dot(
        tri.astype(F32).astype(BF16),
        chosen.astype(F32).astype(BF16),
        preferred_element_type=F32,
    )
    slot = jnp.where(chosen, before, jnp.float32(-1.0))

    for k in range(1, T):
        source = lax.rem(t + k, T)
        remote(
            conv_out.at[source], conv_in.at[source], a2a_send.at[source], a2a_recv.at[source], s, source
        ).wait_recv()
    total = jnp.zeros((rows, 1), F32)
    for j in range(T):
        total = total + jnp.sum(conv_in[j].astype(F32), axis=1, keepdims=True)
    average = total / (T * width)
    total = jnp.zeros((rows, 1), F32)
    for j in range(T):
        centered = conv_in[j].astype(F32) - average
        total = total + jnp.sum(centered * centered, axis=1, keepdims=True)
    scale = lax.rsqrt(total / (T * width) + epsilon)
    for j in range(T):
        cols = slice(j * width, (j + 1) * width)
        v = (conv_in[j].astype(F32) - average) * scale * gain_conv_ref[:, cols] + bias_conv_ref[
            :, cols
        ]
        act[j, :, :] = (v / (1.0 + jnp.exp(-v))).astype(BF16)

    for k in range(1, Z):
        from_z = lax.rem(z - k + Z, Z)
        row = 2 * from_z + core
        for j in range(1, S):
            source = lax.rem(s - j + S, S)
            remote(
                wfull.at[row, source],
                wfull.at[row, source],
                wx_send.at[j, from_z],
                wx_recv.at[source, from_z],
                source,
                t,
            ).wait_recv()
        c = remote(
            wfull.at[row], wfull.at[row], wp_send.at[from_z], wp_recv.at[from_z], s, partner
        )
        c.start()
        waits.append(c)
    loads[2].wait()
    for j in range(Z):
        row = 2 * j + 1 - core
        remote(wfull.at[row], wfull.at[row], wp_send.at[j], wp_recv.at[j], s, partner).wait_recv()

    def project(j, squares):
        cols = pl.ds(pl.multiple_of(j * piece, piece), piece)
        acc = residual[:, cols].astype(F32)
        part = jnp.zeros_like(acc)
        for i in range(T):
            part = part + jnp.dot(act[i], wfull[i, j], preferred_element_type=F32)
        state = (acc + part).astype(BF16)
        hidden[:, cols] = state
        state = state.astype(F32)
        return squares + jnp.sum(state * state, axis=1, keepdims=True)

    squares = lax.fori_loop(0, S, project, jnp.zeros((rows, 1), F32))
    scale = lax.rsqrt(squares / D + epsilon)

    def norm_cols(j, _):
        cols = pl.ds(pl.multiple_of(j * piece, piece), piece)
        normed[:, cols] = (hidden[:, cols].astype(F32) * scale * gain_moe_ref[:, cols]).astype(BF16)
        return 0

    lax.fori_loop(0, S, norm_cols, 0)

    slot_iota = lax.broadcasted_iota(jnp.int32, (rows, cap), 1).astype(F32)

    def column(array, expert):
        return jnp.sum(
            jnp.where(lane == expert + G, array, jnp.float32(0.0)), axis=1, keepdims=True
        )

    def gather_rows(expert, target):
        picks = (column(slot, expert) == slot_iota).astype(F32).astype(BF16)

        def cols_step(j, _):
            cols = pl.ds(pl.multiple_of(j * piece, piece), piece)
            target[:, cols] = lax.dot_general(
                picks,
                normed[:, cols],
                (((0,), (0,)), ((), ())),
                preferred_element_type=F32,
            ).astype(BF16)
            return 0

        lax.fori_loop(0, S, cols_step, 0)

    for k in range(1, S):
        expert = lax.rem(s + k, S)
        gather_rows(expert, outgoing.at[expert])
        remote(
            outgoing.at[expert], arrived.at[s], disp_send.at[expert], disp_recv.at[s], expert, t
        ).start()
    gather_rows(s, arrived.at[s])

    logits = jnp.dot(normed[...], router_ref[...], preferred_element_type=F32)
    exps = jnp.exp(logits)
    zero = jnp.float32(0.0)
    group_prob = jnp.sum(jnp.where(in_group, exps, zero), axis=1, keepdims=True) / jnp.sum(
        jnp.where(lane < G, exps, zero), axis=1, keepdims=True
    )
    chosen_exp = jnp.where(chosen, exps, zero)
    mix = group_prob * chosen_exp / jnp.sum(chosen_exp, axis=1, keepdims=True)

    for c in loads[3:]:
        c.wait()
    ff = gate_w.shape[2]
    ff_step = min(ff, 256)

    def expert_block(sender, target):
        def up_step(j, _):
            cols = pl.ds(pl.multiple_of(j * ff_step, ff_step), ff_step)
            x = arrived[sender]
            g = jnp.dot(x, gate_w[0, :, cols], preferred_element_type=F32)
            u = jnp.dot(x, up_w[0, :, cols], preferred_element_type=F32)
            ffn_hidden[:, cols] = (g / (1.0 + jnp.exp(-g)) * u).astype(BF16)
            return 0

        lax.fori_loop(0, ff // ff_step, up_step, 0)

        def down_step(j, _):
            cols = pl.ds(pl.multiple_of(j * piece, piece), piece)
            target[:, cols] = jnp.dot(
                ffn_hidden[...], down_w[0, :, cols], preferred_element_type=F32
            ).astype(BF16)
            return 0

        lax.fori_loop(0, S, down_step, 0)

    expert_block(s, returned.at[s])
    for k in range(1, S):
        sender = lax.rem(s - k + S, S)
        remote(
            outgoing.at[sender], arrived.at[sender], disp_send.at[sender], disp_recv.at[sender], sender, t
        ).wait_recv()
        expert_block(sender, results.at[sender])
        remote(
            results.at[sender], returned.at[s], ret_send.at[sender], ret_recv.at[s], sender, t
        ).start()

    for k in range(1, S):
        expert = lax.rem(s + k, S)
        remote(
            results.at[expert], returned.at[expert], ret_send.at[expert], ret_recv.at[expert], expert, t
        ).wait_recv()
    spreads = [
        jnp.where(column(slot, e) == slot_iota, column(mix, e), zero).astype(BF16)
        for e in range(E)
    ]

    def combine(j, _):
        cols = pl.ds(pl.multiple_of(j * piece, piece), piece)
        acc = jnp.zeros((rows, piece), F32)
        for e in range(E):
            acc = acc + jnp.dot(spreads[e], returned[e, :, cols], preferred_element_type=F32)
        out_ref[:, cols] = (hidden[:, cols].astype(F32) + acc).astype(BF16)
        return 0

    lax.fori_loop(0, S, combine, 0)

    for c in waits:
        c.wait_send()
    rim_done = None
    for k in range(1, T):
        to = lax.rem(t + k, T)
        remote(conv_out.at[to], conv_in.at[t], a2a_send.at[to], a2a_recv.at[t], s, to).wait_send()
    for k in range(1, S):
        to = lax.rem(s + k, S)
        remote(outgoing.at[to], arrived.at[s], disp_send.at[to], disp_recv.at[s], to, t).wait_send()
        remote(results.at[to], returned.at[s], ret_send.at[to], ret_recv.at[s], to, t).wait_send()


def body(
    S,
    T,
    conv_value,
    conv_gate,
    doc_ids,
    conv_kernel,
    norm_gain_conv,
    norm_bias_conv,
    proj_weight,
    residual,
    norm_gain_moe,
    group_router,
    expert_router,
    routing,
    expert_gate_w,
    expert_up_w,
    expert_down_w,
):
    tokens, width = conv_value.shape
    n_taps = conv_kernel.shape[0]
    rows, D = residual.shape
    wrows = proj_weight.shape[0]
    ff = expert_gate_w.shape[2]
    G = group_router.shape[1]
    E = expert_router.shape[1]
    cap = 2 * rows // E
    lanes = min(width, 128)
    start = jnp.sum((doc_ids[None, :] < doc_ids[:, None]).astype(jnp.int32), axis=1)
    position = jnp.arange(tokens, dtype=jnp.int32)
    least = jnp.where(start == 0, 0, n_taps - 1 - (position - start))
    least_tap = jnp.broadcast_to(least[:, None], (tokens, lanes))
    last_id = doc_ids[tokens - 1]
    rim_keep = jnp.broadcast_to(
        (doc_ids[tokens - HALO :] == last_id).astype(F32)[:, None], (HALO, width)
    )
    last_ids = jnp.full((16, width), last_id.astype(BF16))
    first_ids = jnp.full((16, width), doc_ids[0].astype(F32))
    router = jnp.concatenate(
        [group_router, expert_router, jnp.zeros((D, 128 - G - E), BF16)], axis=1
    )
    vmem = pl.BlockSpec(memory_space=pltpu.VMEM)
    hbm = pl.BlockSpec(memory_space=pl.ANY)
    dma = pltpu.SemaphoreType.DMA
    piece = D // S
    Z = T // 2
    return pl.pallas_call(
        functools.partial(kernel, S, T, G),
        out_shape=jax.ShapeDtypeStruct((rows, D), BF16),
        in_specs=[
            hbm, hbm, vmem, vmem, vmem, vmem, vmem, vmem, vmem, hbm, hbm, vmem, vmem, vmem,
            hbm, hbm, hbm,
        ],
        out_specs=vmem,
        scratch_shapes=[
            pltpu.VMEM((tokens, width), BF16),
            pltpu.VMEM((tokens, width), BF16),
            pltpu.VMEM((T, S, wrows, piece), BF16),
            pltpu.VMEM((rows, D), BF16),
            pltpu.VMEM((1, D, ff), BF16),
            pltpu.VMEM((1, D, ff), BF16),
            pltpu.VMEM((1, ff, D), BF16),
            pltpu.VMEM((HALO + 16, width), BF16),
            pltpu.VMEM((HALO + 16, width), BF16),
            pltpu.VMEM((tokens + HALO, width), F32),
            pltpu.VMEM((32, width), F32),
            pltpu.VMEM((T, rows, width), BF16),
            pltpu.VMEM((T, rows, width), BF16),
            pltpu.VMEM((T, rows, width), BF16),
            pltpu.VMEM((rows, D), BF16),
            pltpu.VMEM((rows, D), BF16),
            pltpu.VMEM((E, cap, D), BF16),
            pltpu.VMEM((E, cap, D), BF16),
            pltpu.VMEM((cap, ff), BF16),
            pltpu.VMEM((E, cap, D), BF16),
            pltpu.VMEM((E, cap, D), BF16),
            dma((6,)),
            dma((S,)),
            dma((2,)),
            dma((Z,)),
            dma((Z,)),
            dma((S, Z)),
            dma((S, Z)),
            dma((Z,)),
            dma((Z,)),
            dma((T,)),
            dma((T,)),
            dma((S,)),
            dma((S,)),
            dma((S,)),
            dma((S,)),
        ],
        compiler_params=pltpu.CompilerParams(
            collective_id=0, has_side_effects=True, vmem_limit_bytes=60 * 1024 * 1024
        ),
    )(
        conv_value,
        conv_gate,
        least_tap,
        rim_keep,
        last_ids,
        first_ids,
        conv_kernel,
        norm_gain_conv[None, :],
        norm_bias_conv[None, :],
        proj_weight,
        residual,
        norm_gain_moe[None, :],
        router,
        routing,
        expert_gate_w,
        expert_up_w,
        expert_down_w,
    )


def solution(mesh):
    placed = (
        P("sp", "tp"),
        P("sp", "tp"),
        P("sp"),
        P(None, "tp"),
        P(),
        P(),
        P("tp", None),
        P(("sp", "tp"), None),
        P(),
        P(),
        P(),
        P(("sp", "tp"), None),
        P("sp", None, None),
        P("sp", None, None),
        P("sp", None, None),
    )
    return jax.shard_map(
        functools.partial(body, mesh.shape["sp"], mesh.shape["tp"]),
        mesh=mesh,
        in_specs=placed,
        out_specs=P(("sp", "tp"), None),
        check_vma=False,
    )
```

time: 170 us -> 122 us (0.72)
  Pallas kernels: 0 us -> 105 us
  waiting for transfers between devices: 68.7 us -> 0 us
  blocking collectives: 23 us -> 0 us
  other arithmetic: 22.7 us -> 4.3 us
  matrix products: 17.6 us -> 0 us
  starting transfers between devices: 14.2 us -> 0 us
  between operations: 14.9 us -> 1.24 us
    pallas_call x0 -> x1, Pallas kernels: none -> 105 us  [body(): pl.pallas_call(functools.partial(kernel, S, T, G), out_shape=jax.ShapeDty...]
    all_to_all x2 -> x0, waiting for transfers between devices: 46.8 us -> none  [the longest x1 28.8 us: body(): lax.all_to_all(convolved, 'tp', split_axis=0, concat_axis=1, tiled=True)]
    all_to_all x1 -> x0, blocking collectives: 23 us -> none  [body(): lax.all_to_all(outgoing, 'sp', split_axis=0, concat_axis=0, tiled=True)]
    all_gather x1 -> x0, waiting for transfers between devices: 20.5 us -> none  [body(): weight_full = lax.all_gather(weight_piece, ('sp', 'tp'), axis=0, tiled=True)]
    dot_general x8 -> x0, matrix products: 17.6 us -> none  [the longest x1 5.46 us: body(): jnp.dot(reordered, weight_full, preferred_element_type=jnp.float32)]
    convert_element_type x5 -> x1, other arithmetic: 18 us -> 1.32 us  [body(): (doc_ids[tokens - HALO:] == last_id).astype(F32)[:, None]]
    all_to_all x2 -> x0, starting transfers between devices: 9.35 us -> none  [the longest x1 4.88 us: body(): lax.all_to_all(convolved, 'tp', split_axis=0, concat_axis=1, tiled=True)]
    ppermute x1 -> x0, starting transfers between devices: 4.87 us -> none  [halo(): return lax.ppermute(jnp.concatenate([rim, id_row], axis=0), 'sp', pairs)]
  transfers between devices with their start and end apart: 4 -> 0, of which waited for: 4 -> 0; matrix products, arithmetic and copies ran while one was open for 17% -> 0% of each run, Pallas kernels for 0% -> 0%
where the time goes in v2:
time: 122 us; the launch traced here: 120 us
  Pallas kernels  105 us (86%)
  local copies, waits for them, and re-layouts  9.94 us (8%)
  other arithmetic  4.3 us (4%)
  between operations  1.24 us (1%)
    pallas_call x1, Pallas kernels, body(): pl.pallas_call(functools.partial(kernel, S, T, G), out_shape=jax.ShapeDty...  105 us
    unnamed x4, local copies, waits for them, and re-layouts  5.56 us

profile of v2, /device:TPU:0, one launch (start us, length us, event | category | flops | bytes accessed | tf_op | source)
XLA Modules:
  0.0 120.2 jit_solution(14592033327679910581)
XLA Ops:
  0.0 0.1 pad.2.clone
  0.1 1.3 %fusion = (s32[1]{0:T(128)}, s32[1]{0:T(128)}) fusion(s32[1536]{0:T(1024)} %param.17), kind=kLoop, calls=%fused_computation.4 | loop fusion | bytes 16 | tf_op jit(solution)/shard_map/slice | solution.py:461
  2.6 1.3 %compare_convert_fusion = f32[32]{0:T(128)S(1)} fusion(s32[1536]{0:T(1024)} %param.17, s32[]{:T(128)} %bitcast), kind=kLoop, calls=%fused_computation.3 | loop fusion | flops 64 | bytes 260 | tf_op jit(solution)/shard_map/convert_element_type | solution.py:458
  3.9 0.6 broadcast_in_dim.36.last_id_ref
  4.5 1.8 %convert_reduce_fusion = s32[1536]{0:T(1024)S(1)} fusion(s32[1536]{0:T(1024)} %param.17), kind=kLoop, calls=%fused_computation | loop fusion | flops 7076352 | bytes 12288 | tf_op jit(solution)/shard_map/reduce_sum | solution.py:452
  6.4 0.6 broadcast_in_dim.37.first_id_ref
  7.0 0.7 broadcast_in_dim.35.rim_keep_ref
  7.6 1.4 %copy.21.routing_ref = s32[192,2]{1,0:T(8,128)} copy(s32[192,2]{0,1:T(2,128)} %param.26) | data formatting | bytes 3072 | tf_op args[11]
  9.1 1.0 copy.19
  10.1 1.0 copy.20
  11.1 1.1 maximum_maximum_fusion.router_ref
  12.2 1.1 broadcast_in_dim.34.least_tap_ref
  13.4 104.8 %shard_map.145 = bf16[192,2048]{1,0:T(8,128)(2,1)} custom-call(bf16[1536,256]{1,0:T(8,128)(2,1)} %value_hbm.1, bf16[1536,256]{1,0:T(8,128)(2,1)} %gate_hbm.1, s32[1536,128]{1,0:T(8,128)} %broadcast_in_dim.34.least_tap_ref, f32[32,256]{1,0:T(8,128)} %broadcast_in_dim.35.rim_keep_ref, bf16[16,256]{1,0:T(8,128)(2,1)} %broadcast_in_dim.36.last_id_ref, ...), custom_call_target="tpu_custom_call" | custom-call | tf_op jit(solution)/shard_map/pallas_call | solution.py:470
  118.2 2.1 %copy.23 = bf16[192,2048]{1,0:T(8,128)(2,1)} copy(bf16[192,2048]{1,0:T(8,128)(2,1)} %shard_map.145) | data formatting | bytes 1572864
  (2 shorter events, 0.0 us)

commit v3 on v2

--- a/solution.py
+++ b/solution.py
@@ -25,16 +25,15 @@
     value_hbm,
     gate_hbm,
     least_tap_ref,
-    rim_keep_ref,
-    last_id_ref,
-    first_id_ref,
+    ids_ref,
     kernel_ref,
     gain_conv_ref,
     bias_conv_ref,
     weight_hbm,
     residual_hbm,
     gain_moe_ref,
-    router_ref,
+    group_router_ref,
+    expert_router_ref,
     routing_ref,
     gate_w_hbm,
     up_w_hbm,
@@ -151,9 +150,13 @@
     loads[0].wait()
     loads[1].wait()
     tail = pl.ds(tokens - HALO, HALO)
-    rim = gate(value[tail, :], gates[tail, :]).astype(F32) * rim_keep_ref[...]
+    last_reach = jnp.max(least_tap_ref[tokens - 1 : tokens, :], axis=1, keepdims=True)
+    newer = lax.broadcasted_iota(jnp.int32, (HALO, width), 0) >= last_reach + HALO - n_taps
+    rim = jnp.where(newer, gate(value[tail, :], gates[tail, :]).astype(F32), jnp.float32(0.0))
     rim_out[0:HALO, :] = rim.astype(BF16)
-    rim_out[HALO : HALO + 16, :] = last_id_ref[...]
+    rim_out[HALO : HALO + 16, :] = jnp.full(
+        (16, width), ids_ref[tokens - 1].astype(F32), F32
+    ).astype(BF16)
     rim_copy = remote(
         rim_out, rim_in, rim_sem.at[0], rim_sem.at[1], lax.rem(s + 1, S), t
     )
@@ -168,7 +171,7 @@
     lax.fori_loop(0, tokens // 64, gate_rows, 0)
     taps[0:n_taps, :] = kernel_ref[...].astype(F32)
     rim_copy.wait()
-    same = (rim_in[HALO : HALO + 1, :].astype(F32) == first_id_ref[0:1, :]) & (s > 0)
+    same = (rim_in[HALO : HALO + 1, :].astype(F32) == ids_ref[0].astype(F32)) & (s > 0)
     padded[0:HALO, :] = jnp.where(same, rim_in[0:HALO, :].astype(F32), jnp.float32(0.0))
 
     step_rows = 32 if block % 32 == 0 else 8
@@ -209,11 +212,11 @@
         ).start()
         return 0
 
-    lax.fori_loop(1, T, conv_send, 0)
-    conv_block(t)
-    conv_in[t, :, :] = conv_out[t, :, :]
-
+    done = 1
     for k in range(1, Z):
+        upto = T - 2 * (Z - 1 - k)
+        lax.fori_loop(done, upto, conv_send, 0)
+        done = upto
         from_z = lax.rem(z - k + Z, Z)
         row = 2 * from_z + core
         remote(
@@ -230,15 +233,29 @@
             )
             c.start()
             waits.append(c)
+    conv_block(t)
+    conv_in[t, :, :] = conv_out[t, :, :]
 
     rows = block
     E = S
     cap = 2 * rows // E
     lane = lax.broadcasted_iota(jnp.int32, (rows, 128), 1)
-    first = routing_ref[:, 0:1]
-    second = routing_ref[:, 1:2]
-    chosen = (lane == first + G) | (lane == second + G)
-    in_group = lane == first // (E // G)
+    eye = lax.broadcasted_iota(jnp.int32, (rows, rows), 0) == lax.broadcasted_iota(
+        jnp.int32, (rows, rows), 1
+    )
+    named = lax.dot_general(
+        eye.astype(F32).astype(BF16),
+        routing_ref[...].astype(F32).astype(BF16),
+        (((1,), (1,)), ((), ())),
+        preferred_element_type=F32,
+    )
+    first = named[:, 0:1]
+    second = named[:, 1:2]
+    lane_f = lane.astype(F32)
+    chosen = (lane_f == first) | (lane_f == second)
+    per_group = E // G
+    group_low = lane_f * per_group
+    in_group = (first >= group_low) & (first < group_low + per_group)
     tri = lax.broadcasted_iota(jnp.int32, (rows, rows), 0) > lax.broadcasted_iota(
         jnp.int32, (rows, rows), 1
     )
@@ -317,9 +334,8 @@
     slot_iota = lax.broadcasted_iota(jnp.int32, (rows, cap), 1).astype(F32)
 
     def column(array, expert):
-        return jnp.sum(
-            jnp.where(lane == expert + G, array, jnp.float32(0.0)), axis=1, keepdims=True
-        )
+        mine = lane[:, : array.shape[1]] == expert
+        return jnp.sum(jnp.where(mine, array, jnp.float32(0.0)), axis=1, keepdims=True)
 
     def gather_rows(expert, target):
         picks = (column(slot, expert) == slot_iota).astype(F32).astype(BF16)
@@ -344,13 +360,18 @@
         ).start()
     gather_rows(s, arrived.at[s])
 
-    logits = jnp.dot(normed[...], router_ref[...], preferred_element_type=F32)
-    exps = jnp.exp(logits)
+    def logits(router):
+        return lax.dot_general(
+            normed[...], router[...], (((1,), (1,)), ((), ())), preferred_element_type=F32
+        )
+
+    group_exp = jnp.exp(logits(group_router_ref))
+    expert_exp = jnp.exp(logits(expert_router_ref))
     zero = jnp.float32(0.0)
-    group_prob = jnp.sum(jnp.where(in_group, exps, zero), axis=1, keepdims=True) / jnp.sum(
-        jnp.where(lane < G, exps, zero), axis=1, keepdims=True
-    )
-    chosen_exp = jnp.where(chosen, exps, zero)
+    group_prob = jnp.sum(
+        jnp.where(in_group[:, :G], group_exp, zero), axis=1, keepdims=True
+    ) / jnp.sum(group_exp, axis=1, keepdims=True)
+    chosen_exp = jnp.where(chosen[:, :E], expert_exp, zero)
     mix = group_prob * chosen_exp / jnp.sum(chosen_exp, axis=1, keepdims=True)
 
     for c in loads[3:]:
@@ -411,7 +432,6 @@
 
     for c in waits:
         c.wait_send()
-    rim_done = None
     for k in range(1, T):
         to = lax.rem(t + k, T)
         remote(conv_out.at[to], conv_in.at[t], a2a_send.at[to], a2a_recv.at[t], s, to).wait_send()
@@ -453,17 +473,9 @@
     position = jnp.arange(tokens, dtype=jnp.int32)
     least = jnp.where(start == 0, 0, n_taps - 1 - (position - start))
     least_tap = jnp.broadcast_to(least[:, None], (tokens, lanes))
-    last_id = doc_ids[tokens - 1]
-    rim_keep = jnp.broadcast_to(
-        (doc_ids[tokens - HALO :] == last_id).astype(F32)[:, None], (HALO, width)
-    )
-    last_ids = jnp.full((16, width), last_id.astype(BF16))
-    first_ids = jnp.full((16, width), doc_ids[0].astype(F32))
-    router = jnp.concatenate(
-        [group_router, expert_router, jnp.zeros((D, 128 - G - E), BF16)], axis=1
-    )
     vmem = pl.BlockSpec(memory_space=pltpu.VMEM)
     hbm = pl.BlockSpec(memory_space=pl.ANY)
+    smem = pl.BlockSpec(memory_space=pltpu.SMEM)
     dma = pltpu.SemaphoreType.DMA
     piece = D // S
     Z = T // 2
@@ -471,7 +483,7 @@
         functools.partial(kernel, S, T, G),
         out_shape=jax.ShapeDtypeStruct((rows, D), BF16),
         in_specs=[
-            hbm, hbm, vmem, vmem, vmem, vmem, vmem, vmem, vmem, hbm, hbm, vmem, vmem, vmem,
+            hbm, hbm, vmem, smem, vmem, vmem, vmem, hbm, hbm, vmem, vmem, vmem, vmem,
             hbm, hbm, hbm,
         ],
         out_specs=vmem,
@@ -520,17 +532,16 @@
         conv_value,
         conv_gate,
         least_tap,
-        rim_keep,
-        last_ids,
-        first_ids,
+        doc_ids,
         conv_kernel,
         norm_gain_conv[None, :],
         norm_bias_conv[None, :],
         proj_weight,
         residual,
         norm_gain_moe[None, :],
-        router,
-        routing,
+        group_router.T,
+        expert_router.T,
+        routing.T,
         expert_gate_w,
         expert_up_w,
         expert_down_w,

time: 122 us -> 109 us (0.89)
  the two profiles are of different devices: /device:TPU:0 before, /device:TPU:8 now
where the time goes in v3:
time: 109 us
  Pallas kernels  104 us (95%)
  local copies, waits for them, and re-layouts  3.24 us (3%)
  other arithmetic  1.85 us (2%)
    pallas_call x1, Pallas kernels, body(): pl.pallas_call(functools.partial(kernel, S, T, G), out_shape=jax.ShapeDty...  104 us

profile of v3, /device:TPU:8, one launch (start us, length us, event | category | flops | bytes accessed | tf_op | source)
XLA Modules:
  0.0 108.6 jit_solution(16491196680561118078)
XLA Ops:
  0.0 1.8 %convert_reduce_fusion = s32[1536]{0:T(1024)S(1)} fusion(s32[1536]{0:T(1024)} %ids_ref.1), kind=kLoop, calls=%fused_computation | loop fusion | flops 7076352 | bytes 12288 | tf_op jit(solution)/shard_map/reduce_sum | solution.py:472
  1.9 1.1 %broadcast_in_dim.10.least_tap_ref = s32[1536,128]{1,0:T(8,128)} broadcast(s32[1536]{0:T(1024)S(1)} %subtract_select_fusion), dimensions={0} | broadcast | bytes 792576 | tf_op jit(solution)/shard_map/broadcast_in_dim | solution.py:475
  3.0 103.5 %shard_map.145 = bf16[192,2048]{1,0:T(8,128)(2,1)} custom-call(bf16[1536,256]{1,0:T(8,128)(2,1)} %value_hbm.1, bf16[1536,256]{1,0:T(8,128)(2,1)} %gate_hbm.1, s32[1536,128]{1,0:T(8,128)} %broadcast_in_dim.10.least_tap_ref, s32[1536]{0:T(1024)} %ids_ref.1, bf16[31,256]{1,0:T(8,128)(2,1)} %kernel_ref.1, f32[1,2048]{1,0:T(1,128)} %bitcast.7, ...), custom_call_target="tpu_custom_call" | custom-call | tf_op jit(solution)/shard_map/pallas_call | solution.py:482
  106.6 2.1 %copy.17 = bf16[192,2048]{1,0:T(8,128)(2,1)} copy(bf16[192,2048]{1,0:T(8,128)(2,1)} %shard_map.145) | data formatting | bytes 1572864
  (1 shorter events, 0.0 us)
